TPU v7x, 32 devices: a whole 2x2x4 slice. The times are simulated.
32 devices in a mesh: sp: 16 (over z, y, x), tp: 2 (over core).
Axes of the slice: x: 2, y: 2, z: 4, core: 2. Of those that a mesh axis runs over, the one named last changes fastest.
Arguments:
- tokens: bfloat16 [4096, 2048], P('sp'), may hold values from -6 to 6
- ln_gain: float32 [2048], replicated, may hold values from 0.1 to 1.9
- w_query_attn: bfloat16 [2048, 1024], P('sp', 'tp'), may hold values from -0.125 to 0.125
- w_key_attn: bfloat16 [2048, 1024], P('sp', 'tp'), may hold values from -0.125 to 0.125
- w_value_attn: bfloat16 [2048, 1024], P('sp', 'tp'), may hold values from -0.125 to 0.125
- w_query_delta: bfloat16 [2048, 1024], P('sp', 'tp'), may hold values from -0.125 to 0.125
- w_key_delta: bfloat16 [2048, 1024], P('sp', 'tp'), may hold values from -0.125 to 0.125
- w_value_delta: bfloat16 [2048, 1024], P('sp', 'tp'), may hold values from -0.125 to 0.125
- w_beta: bfloat16 [2048, 8], replicated, may hold values from -0.125 to 0.125
- w_decay: bfloat16 [2048, 8], replicated, may hold values from -0.125 to 0.125
- attn_bias: float32 [16], replicated, may hold values from -13 to 1
- decay_log: float32 [8], replicated, may hold values from -15 to -2
- beta_bias: float32 [8], replicated, may hold values from -7 to 1
- log_decay_extra: float32 [4096, 8], P('sp', 'tp'), may hold values from -0.7 to 0, as said below
- attn_gain: float32 [64], replicated, may hold values from 0.1 to 1.9
- delta_gain: float32 [128], replicated, may hold values from 0.1 to 1.9
- w_out_attn: bfloat16 [1024, 2048], P('tp', 'sp'), may hold values from -0.125 to 0.125
- w_out_delta: bfloat16 [1024, 2048], P('tp', 'sp'), may hold values from -0.125 to 0.125
Outputs:
- mixed_out: bfloat16 [4096, 2048], P(('sp', 'tp'))
Inputs may be any that keep to these rules, and one draw needn't show every extreme that they name: `log_decay_extra`: never positive.
All inputs are finite; a program needn't handle non-finite values.
Results may differ from a plain program's by a relative error of at most 0.015.
Values may be sent and summed in bfloat16 or wider, within the bound.
A program may use at most 192 MiB of HBM per device.

v0:
```python
import math

import jax
import jax.numpy as jnp
from jax import lax
from jax.sharding import PartitionSpec as P

SB_DIM = 64
GDN_DIM = 128
DBLOCK = 64


precise = lax.Precision.HIGHEST


def from_behind(value, axis, by):
    length = lax.axis_size(axis)
    pairs = [(i, i + by) for i in range(length) if 0 <= i + by < length]
    return lax.ppermute(value, axis, pairs)


def carried_in(value, axis, join, neutral):
    count, mine = (lax.axis_size(axis), lax.axis_index(axis))
    pieces = jax.tree.map(lambda part: lax.all_gather(part, axis), value)
    running = jax.tree.map(
        lambda part, zero: jnp.full_like(part, 0) + jnp.asarray(zero, part.dtype), value, neutral
    )

    def turn(position, running):
        longer = join(running, jax.tree.map(lambda part: part[position], pieces))
        return jax.tree.map(lambda new, old: jnp.where(position < mine, new, old), longer, running)

    return lax.fori_loop(0, count - 1, turn, running)


def layer_normed(tok_rows, ln_gain):
    values = tok_rows.astype(jnp.float32)
    center = jnp.mean(values, axis=-1, keepdims=True)
    spread = jnp.mean(jnp.square(values - center), axis=-1, keepdims=True)
    return ((values - center) * lax.rsqrt(spread + 1e-05) * ln_gain).astype(jnp.bfloat16)


def rms_scaled(values, gain):
    return values * lax.rsqrt(jnp.mean(jnp.square(values), axis=-1, keepdims=True) + 1e-06) * gain


def unit_rows(values):
    return values * lax.rsqrt(jnp.sum(jnp.square(values), axis=-1, keepdims=True) + 1e-06)


def stick_block(carry, queries, query_pos, head_bias, key_block, value_block, key_first):
    outputs, log_kept = carry
    key_count = key_block.shape[0]
    heads = queries.shape[1]
    head_width = queries.shape[2]
    scores = jnp.einsum(
        "rhd,khd->hrk",
        queries,
        key_block.reshape(key_count, heads, head_width),
        preferred_element_type=jnp.float32,
    )
    scores = scores * head_width ** (-0.5) + head_bias[:, None, None]
    key_pos = key_first + jnp.arange(key_count, dtype=jnp.int32)
    visible = (key_pos[None, :] < query_pos[:, None]) & (key_pos[None, :] >= 0)
    lost = jnp.where(visible[None], -jax.nn.softplus(scores), 0.0)
    between = lax.cumsum(lost, axis=2, reverse=True) - lost + log_kept[:, :, None]
    weights = jnp.where(visible[None], jnp.exp(jax.nn.log_sigmoid(scores) + between), 0.0).astype(
        jnp.bfloat16
    )
    outputs = outputs + jnp.einsum(
        "hrk,khd->hrd",
        weights,
        value_block.reshape(key_count, heads, head_width),
        preferred_element_type=jnp.float32,
    )
    return (outputs, log_kept + jnp.sum(lost, axis=2))


def stick_span(carry, queries, query_pos, head_bias, keys, values, key_first):
    own_rows = queries.shape[0]
    length = keys.shape[0]
    widest = max(1, 1024 // own_rows)
    widest = 1 << widest.bit_length() - 1
    block = own_rows * math.gcd(widest, length // own_rows)
    if length <= block:
        return stick_block(carry, queries, query_pos, head_bias, keys, values, key_first)
    blocks = length // block

    def one_turn(step_index, inner):
        block_index = blocks - 1 - step_index
        key_block = lax.dynamic_slice_in_dim(keys, block_index * block, block, 0)
        value_block = lax.dynamic_slice_in_dim(values, block_index * block, block, 0)
        return stick_block(
            inner,
            queries,
            query_pos,
            head_bias,
            key_block,
            value_block,
            key_first + block_index * block,
        )

    return lax.fori_loop(0, blocks, one_turn, carry)


def delta_parts(queries, keys, values, beta, decay):
    width = queries.shape[-2]
    key_width = queries.shape[-1]
    decay_sum = jnp.cumsum(decay, axis=-1)
    lower = jnp.tril(jnp.ones((width, width), dtype=bool))
    strict = jnp.tril(jnp.ones((width, width), dtype=bool), -1)
    differ = decay_sum[..., :, None] - decay_sum[..., None, :]
    decay_mask = jnp.where(lower, jnp.exp(jnp.where(lower, differ, 0.0)), 0.0)
    keys_beta = keys * beta[..., None]
    values_beta = values * beta[..., None]
    strict_mat = jnp.where(
        strict,
        jnp.einsum("...id,...jd->...ij", keys_beta, keys, precision=precise) * decay_mask,
        0.0,
    )
    right_side = jnp.concatenate([keys_beta * jnp.exp(decay_sum)[..., None], values_beta], axis=-1)
    solved = jax.scipy.linalg.solve_triangular(
        jnp.eye(width, dtype=jnp.float32) + strict_mat, right_side, lower=True
    )
    solve_keys = solved[..., :key_width]
    solve_values = solved[..., key_width:]
    query_key = jnp.einsum("...id,...jd->...ij", queries, keys, precision=precise) * decay_mask
    query_decayed = queries * jnp.exp(decay_sum)[..., None]
    keys_to_end = keys * jnp.exp(decay_sum[..., -1:] - decay_sum)[..., None]
    block_decay = jnp.exp(decay_sum[..., -1])
    return (solve_keys, solve_values, query_decayed, query_key, keys_to_end, block_decay)


def delta_update(state, block_parts):
    solve_keys, solve_values, query_decayed, query_key, keys_to_end, block_decay = block_parts
    fresh = solve_values - jnp.einsum("hcd,hde->hce", solve_keys, state, precision=precise)
    outputs = jnp.einsum("hcd,hde->hce", query_decayed, state, precision=precise)
    outputs = outputs + jnp.einsum("hij,hje->hie", query_key, fresh, precision=precise)
    state = state * block_decay[:, None, None] + jnp.einsum(
        "hcd,hce->hde", keys_to_end, fresh, precision=precise
    )
    return (state, outputs)


def chain_combine(earlier, later):
    earlier_map, earlier_state = earlier
    later_map, later_state = later
    joined_map = jnp.einsum("hij,hjk->hik", later_map, earlier_map, precision=precise)
    joined_state = (
        jnp.einsum("hij,hjk->hik", later_map, earlier_state, precision=precise) + later_state
    )
    return (joined_map, joined_state)


def local(
    tokens,
    ln_gain,
    w_query_attn,
    w_key_attn,
    w_value_attn,
    w_query_delta,
    w_key_delta,
    w_value_delta,
    w_beta,
    w_decay,
    attn_bias,
    decay_log,
    beta_bias,
    log_decay_extra,
    attn_gain,
    delta_gain,
    w_out_attn,
    w_out_delta,
):
    row_count = tokens.shape[0]
    normed = layer_normed(tokens, ln_gain)
    segments = (
        lax.all_gather(w_query_attn, "sp", axis=0, tiled=True),
        lax.all_gather(w_key_attn, "sp", axis=0, tiled=True),
        lax.all_gather(w_value_attn, "sp", axis=0, tiled=True),
        lax.all_gather(w_query_delta, "sp", axis=0, tiled=True),
        lax.all_gather(w_key_delta, "sp", axis=0, tiled=True),
        lax.all_gather(w_value_delta, "sp", axis=0, tiled=True),
    )
    summed = tuple(
        (jnp.dot(normed, segment, preferred_element_type=jnp.float32) for segment in segments)
    )
    attn_query, attn_key, attn_value, delta_query, delta_key, delta_value = [
        result.astype(jnp.bfloat16) for result in summed
    ]
    tp_pos = lax.axis_index("tp")
    sp_pos = lax.axis_index("sp")
    attn_heads = attn_query.shape[1] // SB_DIM
    delta_heads = delta_query.shape[1] // GDN_DIM
    positions = sp_pos * row_count + jnp.arange(row_count, dtype=jnp.int32)
    queries = attn_query.reshape(row_count, attn_heads, SB_DIM)
    head_bias = lax.dynamic_slice_in_dim(attn_bias, tp_pos * attn_heads, attn_heads, 0)
    carry = (
        jnp.zeros((attn_heads, row_count, SB_DIM), jnp.float32),
        jnp.zeros((attn_heads, row_count), jnp.float32),
    )
    carry = stick_span(
        carry, queries, positions, head_bias, attn_key, attn_value, sp_pos * row_count
    )
    held_keys = attn_key
    held_values = attn_value
    hop_count = (lax.axis_size("sp") - 1).bit_length()
    for hop_level in range(hop_count):
        distance = 1 << hop_level
        got_keys, got_values = from_behind((held_keys, held_values), "sp", distance)
        got_first = (sp_pos - 2 * distance + 1) * row_count
        carry = stick_span(carry, queries, positions, head_bias, got_keys, got_values, got_first)
        if hop_level + 1 < hop_count:
            held_keys = jnp.concatenate([got_keys, held_keys], axis=0)
            held_values = jnp.concatenate([got_values, held_values], axis=0)
    attn_mixed = rms_scaled(carry[0], attn_gain).astype(jnp.bfloat16)
    head_first = tp_pos * delta_heads
    beta_cols = lax.dynamic_slice_in_dim(w_beta, head_first, delta_heads, 1)
    decay_cols = lax.dynamic_slice_in_dim(w_decay, head_first, delta_heads, 1)
    beta_pre = jnp.dot(normed, beta_cols, preferred_element_type=jnp.float32).astype(jnp.bfloat16)
    decay_pre = jnp.dot(normed, decay_cols, preferred_element_type=jnp.float32).astype(jnp.bfloat16)
    queries = unit_rows(
        jax.nn.silu(delta_query.astype(jnp.float32)).reshape(row_count, delta_heads, GDN_DIM)
    ) * GDN_DIM ** (-0.5)
    keys = unit_rows(
        jax.nn.silu(delta_key.astype(jnp.float32)).reshape(row_count, delta_heads, GDN_DIM)
    )
    values = jax.nn.silu(delta_value.astype(jnp.float32)).reshape(row_count, delta_heads, GDN_DIM)
    beta = jax.nn.sigmoid(
        beta_pre.astype(jnp.float32)
        + lax.dynamic_slice_in_dim(beta_bias, head_first, delta_heads, 0)
    )
    rates = jnp.exp(lax.dynamic_slice_in_dim(decay_log, head_first, delta_heads, 0))
    decay = -rates * jax.nn.softplus(decay_pre.astype(jnp.float32)) + log_decay_extra
    blocks = row_count // DBLOCK

    def to_blocks(array):
        return jnp.moveaxis(array.reshape((blocks, DBLOCK) + array.shape[1:]), 2, 0)

    parts = delta_parts(
        to_blocks(queries), to_blocks(keys), to_blocks(values), to_blocks(beta), to_blocks(decay)
    )
    sequence = tuple((jnp.moveaxis(piece_part, 1, 0) for piece_part in parts))
    eye_mat = jnp.eye(GDN_DIM, dtype=jnp.float32)

    def carry_map(accum, block_parts):
        transition, written = accum
        solve_keys, solve_values, query_decayed, query_key, keys_to_end, block_decay = block_parts
        step_matrix = block_decay[:, None, None] * eye_mat - jnp.einsum(
            "hcd,hce->hde", keys_to_end, solve_keys, precision=precise
        )
        transition = jnp.einsum("hij,hjk->hik", step_matrix, transition, precision=precise)
        written = jnp.einsum("hij,hjk->hik", step_matrix, written, precision=precise)
        written = written + jnp.einsum("hcd,hce->hde", keys_to_end, solve_values, precision=precise)
        return ((transition, written), None)

    neutral = (
        jnp.broadcast_to(eye_mat, (delta_heads, GDN_DIM, GDN_DIM)),
        jnp.zeros((delta_heads, GDN_DIM, GDN_DIM), jnp.float32),
    )
    own_chain, _ = lax.scan(carry_map, neutral, sequence)
    _, incoming = carried_in(own_chain, "sp", chain_combine, neutral)
    _, outputs = lax.scan(delta_update, incoming, sequence)
    delta_raw = jnp.moveaxis(outputs, 0, 1).reshape(delta_heads, row_count, GDN_DIM)
    delta_mixed = rms_scaled(delta_raw, delta_gain).astype(jnp.bfloat16)
    full_attn, full_delta = (
        lax.all_gather(w_out_attn, "sp", axis=1, tiled=True),
        lax.all_gather(w_out_delta, "sp", axis=1, tiled=True),
    )
    attn_weight3 = full_attn.reshape(attn_heads, SB_DIM, full_attn.shape[1])
    delta_weight3 = full_delta.reshape(delta_heads, GDN_DIM, full_delta.shape[1])
    result = jnp.einsum("hrd,hdn->rn", attn_mixed, attn_weight3, preferred_element_type=jnp.float32)
    return lax.psum_scatter(
        (
            result
            + jnp.einsum(
                "hrd,hdn->rn", delta_mixed, delta_weight3, preferred_element_type=jnp.float32
            )
        ).astype(jnp.bfloat16),
        "tp",
        scatter_dimension=0,
        tiled=True,
    )


def solution(mesh):
    in_specs = (
        P("sp", None),
        P(),
        P("sp", "tp"),
        P("sp", "tp"),
        P("sp", "tp"),
        P("sp", "tp"),
        P("sp", "tp"),
        P("sp", "tp"),
        P(),
        P(),
        P(),
        P(),
        P(),
        P("sp", "tp"),
        P(),
        P(),
        P("tp", "sp"),
        P("tp", "sp"),
    )
    out_specs = P(("sp", "tp"), None)
    return jax.shard_map(local, mesh=mesh, in_specs=in_specs, out_specs=out_specs, check_vma=False)
```

profile of v0, /device:TPU:0, one launch (start us, length us, event | category | flops | bytes accessed | tf_op | source)
XLA Modules:
  0.0 1027.9 jit_solution(7675977298971607661)
XLA Ops:
  19.1 54.2 %all-gather.21.cloned.1.call-done = bf16[2048,512]{1,0:T(8,128)(2,1)} async-done(((bf16[128,512]{1,0:T(8,128)(2,1)}), bf16[2048,512]{1,0:T(8,128)(2,1)}) %all-gather.21.cloned.1.call-update) | async-done | bytes 2097168 | tf_op jit(solution)/shard_map/all_gather | solution.py:182
  76.5 58.7 %all-gather.23.cloned.1.call-done = bf16[2048,512]{1,0:T(8,128)(2,1)} async-done(((bf16[128,512]{1,0:T(8,128)(2,1)}), bf16[2048,512]{1,0:T(8,128)(2,1)}) %all-gather.23.cloned.1.call-update) | async-done | bytes 2097168 | tf_op jit(solution)/shard_map/all_gather | solution.py:183
  141.7 79.4 %custom-call.4 = f32[4,4,1,64,64]{3,4,2,1,0:T(8,128)S(1)} custom-call(f32[4,4,1,64,64]{4,3,2,1,0:T(8,128)} %fusion.101), custom_call_target="InvertDiagBlocksLowerTriangular" | custom-call | tf_op jit(solution)/shard_map/jit(_solve_triangular)/vmap(vmap())/triangular_solve | solution.py:122
  222.7 11.1 %while.57 = (s32[]{:T(128)}, f32[4,128,128]{2,1,0:T(8,128)S(1)}, f32[4,128,128]{2,1,0:T(8,128)S(1)}, f32[4,4]{1,0:T(4,128)}, f32[4,4,64,128]{3,2,1,0:T(8,128)S(1...) while((s32[]{:T(128)}, f32[4,128,128]{2,1,0:T(8,128)S(1)}, ...), condition=%wide.region_23.24_spmd.clone, body=%wide.region_22.23_spmd.clone.sunk | while | flops 302284800 | bytes 3541643 | solution.py:261
  242.5 3.9 collective-permute-start
  248.2 19.0 %all-gather.17.cloned.1.call-done = bf16[2048,512]{1,0:T(8,128)(2,1)} async-done(((bf16[128,512]{1,0:T(8,128)(2,1)}), bf16[2048,512]{1,0:T(8,128)(2,1)}) %all-gather.17.cloned.1.call-update) | async-done | bytes 2097168 | tf_op jit(solution)/shard_map/all_gather | solution.py:180
  269.6 4.0 collective-permute-start.1
  273.7 54.9 %all-gather.13.cloned.1.call-done = bf16[2048,512]{1,0:T(8,128)(2,1)} async-done(((bf16[128,512]{1,0:T(8,128)(2,1)}), bf16[2048,512]{1,0:T(8,128)(2,1)}) %all-gather.13.cloned.1.call-update) | async-done | bytes 2097168 | tf_op jit(solution)/shard_map/all_gather | solution.py:178
  331.8 58.7 %all-gather.25.cloned.1.call-done = bf16[2048,512]{1,0:T(8,128)(2,1)} async-done(((bf16[128,512]{1,0:T(8,128)(2,1)}), bf16[2048,512]{1,0:T(8,128)(2,1)}) %all-gather.25.cloned.1.call-update) | async-done | bytes 2097168 | tf_op jit(solution)/shard_map/all_gather | solution.py:181
  404.9 5.2 fusion.92
  414.1 5.1 fusion.90
  421.9 3.4 collective-permute-start.2
  427.1 3.4 collective-permute-start.3
  433.4 5.8 fusion.88
  441.3 9.4 collective-permute-start.4
  452.3 5.3 fusion.159
  457.6 5.5 copy.199
  463.0 10.8 %fusion.164 = f32[8,256,4,128]{1,0,3,2:T(8,128)S(1)} fusion(f32[8,256,4,128]{1,0,3,2:T(8,128)} %bitcast.293), kind=kOutput, calls=%fused_computation.277 | output fusion | flops 133169152 | bytes 8388608 | tf_op jit(solution)/shard_map/reduce-window.4
  476.2 5.4 copy.200
  489.6 3.8 fusion.94
  493.5 7.1 fusion.158
  500.6 5.8 copy.224
  506.4 9.4 copy.170
  515.8 20.8 %fusion.165 = f32[8,256,8,128]{1,2,3,0:T(8,128)S(1)} fusion(f32[8,256,8,128]{1,2,3,0:T(8,128)} %copy.170), kind=kOutput, calls=%fused_computation.278 | output fusion | flops 266338304 | bytes 16777216 | tf_op jit(solution)/shard_map/reduce-window.6
  536.6 3.2 copy-done.4
  541.5 7.6 broadcast_add_fusion.1
  549.1 9.2 copy.171
  558.2 9.3 reduce_window_sum.86
  570.2 6.2 collective-permute-start.6
  581.5 6.5 fusion.95
  588.6 12.4 %fusion.70 = f32[8,256,64]{1,2,0:T(8,128)S(1)} fusion(bf16[1024,8,64]{0,2,1:T(8,128)(2,1)S(1)} %bitcast.298, f32[8,256,1024]{2,1,0:T(8,128)} %reduce_window_sum.86, f32[8,256,1024]{2,1,0:T(8,128)} %copy-done.5, f32[8,256,1024]{2,1,0:T(8,128)} %copy-done.13, f32[8,256]{1,0:T(8,128)S(1)} %get-tuple-element.574, f32[8]{0:T(128)S(1)} %dynamic_slice.76, ...), kind=kOutput, calls=%fused_computation.106 | convolution fusion | flops 299892736 | bytes 27009056 | tf_op jit(solution)/shard_map/hrk,khd->hrd/dot_general | solution.py:70
  602.1 27.7 %collective-permute-done.6 = bf16[2048,512]{1,0:T(8,128)(2,1)} collective-permute-done((bf16[2048,512]{1,0:T(8,128)(2,1)}, bf16[2048,512]{1,0:T(8,128)(2,1)}, u32[]{:S(2)}, u32[]{:S(2)}) %collective-permute-start.6) | collective-permute-done | bytes 2097184 | tf_op jit(solution)/shard_map/ppermute | solution.py:19
  629.8 43.0 %collective-permute-done.7 = bf16[2048,512]{1,0:T(8,128)(2,1)} collective-permute-done((bf16[2048,512]{1,0:T(8,128)(2,1)}, bf16[2048,512]{1,0:T(8,128)(2,1)}, u32[]{:S(2)}, u32[]{:S(2)}) %collective-permute-start.7) | collective-permute-done | bytes 2097184 | tf_op jit(solution)/shard_map/ppermute | solution.py:19
  672.8 141.4 %while.56 = (s32[]{:T(128)}, f32[8,256,64]{1,2,0:T(8,128)}, f32[8,256]{1,0:T(8,128)S(1)}, s32[]{:T(128)}, bf16[2048,512]{1,0:T(8,128)(2,1)}, /*index=5*/bf16[256...) while((s32[]{:T(128)}, f32[8,256,64]{1,2,0:T(8,128)}, ...), condition=%wide.region_18.19_spmd.clone, body=%wide.region_14.18_spmd.clone.sunk | while | flops 877397248 | bytes 143126912 | solution.py:103
  675.6 11.2 %fusion.262 = (f32[8,256]{1,0:T(8,128)S(1)}, f32[8,256,1024]{1,2,0:T(8,128)}, f32[8,1024,256]{2,1,0:T(8,128)}) fusion(f32[8]{0:T(128)S(1)} %get-tuple-element.920, pred[256,1024]{0,1:T(8,128)(4,1)S(1)} %compare_and_fusion.6, bf16[1024,8,64]{0,2,1:T(8,128)(2,1)S(1)} %bitcast.291, bf16[256,8,64]{0,2,1:T(8,128)(2,1)} %get-tuple-element.919), kind=kOutput, calls=%fused_computation.52.clone.1 | convolution fusion | flops 291502080 | bytes 18358304 | tf_op jit(solution)/shard_map/while/body/eval_jaxpr/rhd,khd->hrk/dot_general | solution.py:56
  686.9 24.3 %fusion.263 = f32[8,256,8,128]{1,2,3,0:T(8,128)S(1)} fusion(f32[8,256,8,128]{1,3,2,0:T(8,128)} %bitcast.287), kind=kOutput, calls=%fused_computation.40.clone.1 | output fusion | flops 266338304 | bytes 16777216 | tf_op jit(solution)/shard_map/reduce-window.12
  711.1 3.2 copy-done.2
  714.5 3.9 broadcast_add_fusion.6
  721.1 16.2 %fusion.264 = bf16[8,256,1024]{1,2,0:T(8,128)(2,1)} fusion(f32[8,256,8,128]{1,3,2,0:T(8,128)S(1)} %copy.260, f32[8,1024,256]{2,1,0:T(8,128)} %get-tuple-element.794, f32[8,256]{1,0:T(8,128)S(1)} %get-tuple-element.902, f32[8]{0:T(128)S(1)} %get-tuple-element.920, pred[256,1024]{0,1:T(8,128)(4,1)S(1)} %compare_and_fusion.6), kind=kLoop, calls=%fused_computation.28.clone.1 | loop fusion | flops 48234496 | bytes 21241888 | tf_op jit(solution)/shard_map/while/body/eval_jaxpr/convert_element_type | solution.py:67
  744.6 11.5 %fusion.262 = (f32[8,256]{1,0:T(8,128)S(1)}, f32[8,256,1024]{1,2,0:T(8,128)}, f32[8,1024,256]{2,1,0:T(8,128)}) fusion(f32[8]{0:T(128)S(1)} %get-tuple-element.920, pred[256,1024]{0,1:T(8,128)(4,1)S(1)} %compare_and_fusion.6, bf16[1024,8,64]{0,2,1:T(8,128)(2,1)S(1)} %bitcast.291, bf16[256,8,64]{0,2,1:T(8,128)(2,1)} %get-tuple-element.919), kind=kOutput, calls=%fused_computation.52.clone.1 | convolution fusion | flops 291502080 | bytes 18358304 | tf_op jit(solution)/shard_map/while/body/eval_jaxpr/rhd,khd->hrk/dot_general | solution.py:56
  756.1 24.1 %fusion.263 = f32[8,256,8,128]{1,2,3,0:T(8,128)S(1)} fusion(f32[8,256,8,128]{1,3,2,0:T(8,128)} %bitcast.287), kind=kOutput, calls=%fused_computation.40.clone.1 | output fusion | flops 266338304 | bytes 16777216 | tf_op jit(solution)/shard_map/reduce-window.12
  780.1 3.2 copy-done.2
  783.5 4.0 broadcast_add_fusion.6
  790.2 16.2 %fusion.264 = bf16[8,256,1024]{1,2,0:T(8,128)(2,1)} fusion(f32[8,256,8,128]{1,3,2,0:T(8,128)S(1)} %copy.260, f32[8,1024,256]{2,1,0:T(8,128)} %get-tuple-element.794, f32[8,256]{1,0:T(8,128)S(1)} %get-tuple-element.902, f32[8]{0:T(128)S(1)} %get-tuple-element.920, pred[256,1024]{0,1:T(8,128)(4,1)S(1)} %compare_and_fusion.6), kind=kLoop, calls=%fused_computation.28.clone.1 | loop fusion | flops 48234496 | bytes 21241888 | tf_op jit(solution)/shard_map/while/body/eval_jaxpr/convert_element_type | solution.py:67
  815.5 22.3 %while.58 = (s32[]{:T(128)}, f32[4,128,128]{2,1,0:T(8,128)S(1)}, s32[]{:T(128)}, f32[16,4,128,128]{3,2,1,0:T(8,128)}, f32[16,4,128,128]{3,2,1,0:T(8,128)}, /*index=5*/s32[]{:T(128)}, s32[]{:T(128)}) while((s32[]{:T(128)}, f32[4,128,128]{2,1,0:T(8,128)S(1)}, s32[]{:T(128)}, f32[16,4,128,128]{3,2,1,0:T(8,128)}, ...), condition=%wide.region_25.26_spmd.clone, body=%wide.region_24.25_spmd.clone.sunk | while | flops 100925440 | bytes 1837663 | solution.py:33
  837.7 24.1 %while.55 = (s32[]{:T(128)}, f32[4,128,128]{2,1,0:T(8,128)S(1)}, f32[4,4,64,128]{3,2,0,1:T(8,128)S(1)}, f32[4,4]{1,0:T(4,128)}, f32[4,4,64,128]{3,2,1,0:T(8,128)...) while((s32[]{:T(128)}, f32[4,128,128]{2,1,0:T(8,128)S(1)}, ...), condition=%wide.region_28.29_spmd, body=%wide.region_27.28_spmd.sunk | while | flops 176357376 | bytes 2493593 | solution.py:263
  864.8 3.4 fusion.73
  868.2 152.7 %reduce-scatter.2.cloned.1.call-done = bf16[128,2048]{1,0:T(8,128)(2,1)} async-done(((bf16[256,2048]{1,0:T(8,128)(2,1)}), bf16[128,2048]{1,0:T(8,128)(2,1)}) %reduce-scatter.2.cloned.1.call-update) | async-done | bytes 524304 | tf_op jit(solution)/shard_map/reduce_scatter | solution.py:273
  (332 shorter events, 170.2 us)
Async XLA Ops:
  6.5 8.9 copy-start
  6.5 8.8 copy-start.36
  6.5 8.9 copy-start.34
  6.5 10.5 %copy-start.37 = (f32[8]{0:T(128)S(1)}, f32[8]{0:T(128)}, u32[]{:S(2)}) copy-start(f32[8]{0:T(128)} %param.38) | copy-start | bytes 100
  6.5 10.6 %copy-start.32 = (bf16[2048,8]{0,1:T(8,128)(2,1)S(1)}, bf16[2048,8]{0,1:T(8,128)(2,1)}, u32[]{:S(2)}) copy-start(bf16[2048,8]{0,1:T(8,128)(2,1)} %param.34) | copy-start | bytes 98308
  6.5 66.7 %all-gather.21.cloned.1.call-start = ((), (), s32[]{:S(2)}) async-start(), calls=%async_computation.5 | async-start | bytes 2228224 | tf_op jit(solution)/shard_map/all_gather | solution.py:182
  7.3 128.0 %all-gather.23.cloned.1.call-start = ((), (), s32[]{:S(2)}) async-start(), calls=%async_computation.6 | async-start | bytes 2228224 | tf_op jit(solution)/shard_map/all_gather | solution.py:183
  8.0 231.5 %all-gather.15.cloned.1.call-start = ((), (), s32[]{:S(2)}) async-start(), calls=%async_computation.2 | async-start | bytes 2228224 | tf_op jit(solution)/shard_map/all_gather | solution.py:179
  8.8 258.4 %all-gather.17.cloned.1.call-start = ((), (), s32[]{:S(2)}) async-start(), calls=%async_computation.3 | async-start | bytes 2228224 | tf_op jit(solution)/shard_map/all_gather | solution.py:180
  9.3 319.3 %all-gather.13.cloned.1.call-start = ((), (), s32[]{:S(2)}) async-start(), calls=%async_computation.1 | async-start | bytes 2228224 | tf_op jit(solution)/shard_map/all_gather | solution.py:178
  9.9 380.6 %all-gather.25.cloned.1.call-start = ((), (), s32[]{:S(2)}) async-start(), calls=%async_computation.7 | async-start | bytes 2228224 | tf_op jit(solution)/shard_map/all_gather | solution.py:181
  10.5 804.9 %all-gather.29.cloned.1.call-start = ((), (), s32[]{:S(2)}) async-start(), calls=%async_computation.10 | async-start | bytes 4456448 | tf_op jit(solution)/shard_map/all_gather | solution.py:24
  222.7 14.1 %copy-start.38 = (f32[16]{0:T(128)S(1)}, f32[16]{0:T(128)}, u32[]{:S(2)}) copy-start(f32[16]{0:T(128)} %param.36) | copy-start | bytes 196
  233.9 35.6 %copy-start.11 = (f32[4,4,64,128]{3,2,1,0:T(8,128)}, f32[4,4,64,128]{3,2,1,0:T(8,128)S(1)}, u32[]{:S(2)}) copy-start(f32[4,4,64,128]{3,2,1,0:T(8,128)S(1)} %get-tuple-element.941) | copy-start | bytes 1572868
  233.9 35.6 %copy-start.15 = (f32[4,4,64,128]{3,2,1,0:T(8,128)}, f32[4,4,64,128]{3,2,1,0:T(8,128)S(1)}, u32[]{:S(2)}) copy-start(f32[4,4,64,128]{3,2,1,0:T(8,128)S(1)} %get-tuple-element.944) | copy-start | bytes 1572868
  233.9 35.6 %copy-start.16 = (f32[4,4,64,128]{3,2,1,0:T(8,128)}, f32[4,4,64,128]{3,2,1,0:T(8,128)S(1)}, u32[]{:S(2)}) copy-start(f32[4,4,64,128]{3,2,1,0:T(8,128)S(1)} %get-tuple-element.945) | copy-start | bytes 1572868
  234.6 580.9 %all-gather.31.cloned.1.call-start = ((), (), s32[]{:S(2)}) async-start(), calls=%async_computation.11 | async-start | bytes 4456448 | tf_op jit(solution)/shard_map/all_gather | solution.py:24
  235.3 627.1 %all-gather.27.cloned.1.call-start = ((), (), s32[]{:S(2)}) async-start(), calls=%async_computation.8 | async-start | bytes 2228224 | tf_op jit(solution)/shard_map/all_gather | solution.py:268
  236.1 628.7 %all-gather.19.cloned.1.call-start = ((), (), s32[]{:S(2)}) async-start(), calls=%async_computation.4 | async-start | bytes 2228224 | tf_op jit(solution)/shard_map/all_gather | solution.py:267
  236.7 784.3 %reduce-scatter.2.cloned.1.call-start = ((), (), s32[]{:S(2)}) async-start(), calls=%async_computation.9 | async-start | bytes 1572864 | tf_op jit(solution)/shard_map/reduce_scatter | solution.py:273
  242.5 156.9 %collective-permute-start = (bf16[256,512]{1,0:T(8,128)(2,1)}, bf16[256,512]{1,0:T(8,128)(2,1)}, u32[]{:S(2)}, u32[]{:S(2)}) collective-permute-start(bf16[256,512]{1,0:T(8,128)(2,1)} %convolution_convert_fusion.4), channel_id=1, source_target_pairs={{0,2},{2,4},{4,6},{6,8},{8,10},{10,12},{12,14},{14,16},{16,18},{18... | collective-permute-start | bytes 786440 | tf_op jit(solution)/shard_map/ppermute | solution.py:19
  269.5 155.8 %copy-start.20 = (bf16[256,512]{1,0:T(8,128)(2,1)}, bf16[256,512]{1,0:T(8,128)(2,1)S(1)}, u32[]{:S(2)}) copy-start(bf16[256,512]{1,0:T(8,128)(2,1)S(1)} %convolution_convert_fusion.3) | copy-start | bytes 786436
  269.6 155.8 %collective-permute-start.1 = (bf16[256,512]{1,0:T(8,128)(2,1)S(1)}, bf16[256,512]{1,0:T(8,128)(2,1)}, u32[]{:S(2)}, u32[]{:S(2)}) collective-permute-start(bf16[256,512]{1,0:T(8,128)(2,1)S(1)} %convolution_convert_fusion.3), channel_id=1, source_target_pairs={{0,2},{2,4},{4,6},{6,8},{8,10},{10,12},{12,14},{14,16},{16,18},{18... | collective-permute-start | bytes 786440 | tf_op jit(solution)/shard_map/ppermute | solution.py:19
  393.7 8.5 copy-start.27
  421.9 17.3 %collective-permute-start.2 = (bf16[512,512]{1,0:T(8,128)(2,1)}, bf16[512,512]{1,0:T(8,128)(2,1)S(1)}, u32[]{:S(2)}, u32[]{:S(2)}) collective-permute-start(bf16[512,512]{1,0:T(8,128)(2,1)} %pad_maximum_fusion.4), channel_id=1, source_target_pairs={{0,4},{2,6},{4,8},{6,10},{8,12},{10,14},{12,16},{14,18},{16,20},{1... | collective-permute-start | bytes 1572872 | tf_op jit(solution)/shard_map/ppermute | solution.py:19
  427.1 54.4 %collective-permute-start.3 = (bf16[512,512]{1,0:T(8,128)(2,1)}, bf16[512,512]{1,0:T(8,128)(2,1)S(1)}, u32[]{:S(2)}, u32[]{:S(2)}) collective-permute-start(bf16[512,512]{1,0:T(8,128)(2,1)} %pad_maximum_fusion.5), channel_id=1, source_target_pairs={{0,4},{2,6},{4,8},{6,10},{8,12},{10,14},{12,16},{14,18},{16,20},{1... | collective-permute-start | bytes 1572872 | tf_op jit(solution)/shard_map/ppermute | solution.py:19
  433.4 17.5 %copy-start.31 = (bf16[256,512]{0,1:T(8,128)(2,1)S(1)}, bf16[256,512]{0,1:T(8,128)(2,1)}, u32[]{:S(2)}) copy-start(bf16[256,512]{0,1:T(8,128)(2,1)} %copy.154) | copy-start | bytes 786436
  439.2 13.1 %copy-start.28 = (pred[256,512]{1,0:T(8,128)(4,1)S(1)}, pred[256,512]{1,0:T(8,128)(4,1)}, u32[]{:S(2)}) copy-start(pred[256,512]{1,0:T(8,128)(4,1)} %compare_and_fusion.2) | copy-start | bytes 393220
  441.3 46.9 %collective-permute-start.4 = (bf16[1024,512]{1,0:T(8,128)(2,1)}, bf16[1024,512]{1,0:T(8,128)(2,1)S(1)}, u32[]{:S(2)}, u32[]{:S(2)}) collective-permute-start(bf16[1024,512]{1,0:T(8,128)(2,1)} %pad_maximum_fusion.2), channel_id=1, source_target_pairs={{0,8},{2,10},{4,12},{6,14},{8,16},{10,18},{12,20},{14,22},{16,24},... | collective-permute-start | bytes 3145736 | tf_op jit(solution)/shard_map/ppermute | solution.py:19
  452.3 5.3 copy-start.17
  476.2 5.4 copy-start.21
  483.6 92.9 %collective-permute-start.5 = (bf16[1024,512]{1,0:T(8,128)(2,1)}, bf16[1024,512]{1,0:T(8,128)(2,1)S(1)}, u32[]{:S(2)}, u32[]{:S(2)}) collective-permute-start(bf16[1024,512]{1,0:T(8,128)(2,1)} %pad_maximum_fusion.3), channel_id=1, source_target_pairs={{0,8},{2,10},{4,12},{6,14},{8,16},{10,18},{12,20},{14,22},{16,24},... | collective-permute-start | bytes 3145736 | tf_op jit(solution)/shard_map/ppermute | solution.py:19
  493.5 7.1 copy-start.13
  500.6 5.8 copy-start.5
  567.5 13.9 %copy-start.9 = (f32[8,256,512]{2,1,0:T(8,128)S(1)}, f32[8,256,512]{2,1,0:T(8,128)}, u32[]{:S(2)}) copy-start(f32[8,256,512]{2,1,0:T(8,128)} %get-tuple-element.579) | copy-start | bytes 12582916
  567.5 13.9 %copy-start.18 = (f32[8,256,512]{2,1,0:T(8,128)S(1)}, f32[8,256,512]{2,1,0:T(8,128)}, u32[]{:S(2)}) copy-start(f32[8,256,512]{2,1,0:T(8,128)} %copy-done.17) | copy-start | bytes 12582916
  570.2 59.6 %collective-permute-start.6 = (bf16[2048,512]{1,0:T(8,128)(2,1)}, bf16[2048,512]{1,0:T(8,128)(2,1)}, u32[]{:S(2)}, u32[]{:S(2)}) collective-permute-start(bf16[2048,512]{1,0:T(8,128)(2,1)} %pad_maximum_fusion), channel_id=1, source_target_pairs={{0,16},{2,18},{4,20},{6,22},{8,24},{10,26},{12,28},{14,30},{1,17},... | collective-permute-start | bytes 6291464 | tf_op jit(solution)/shard_map/ppermute | solution.py:19
  578.8 94.0 %collective-permute-start.7 = (bf16[2048,512]{1,0:T(8,128)(2,1)}, bf16[2048,512]{1,0:T(8,128)(2,1)}, u32[]{:S(2)}, u32[]{:S(2)}) collective-permute-start(bf16[2048,512]{1,0:T(8,128)(2,1)} %pad_maximum_fusion.1), channel_id=1, source_target_pairs={{0,16},{2,18},{4,20},{6,22},{8,24},{10,26},{12,28},{14,30},{1,17},... | collective-permute-start | bytes 6291464 | tf_op jit(solution)/shard_map/ppermute | solution.py:19
  581.5 7.1 copy-start.25
  588.5 12.4 %copy-start.19 = (bf16[8,256,256]{1,2,0:T(8,128)(2,1)S(1)}, bf16[8,256,256]{1,2,0:T(8,128)(2,1)}, u32[]{:S(2)}) copy-start(bf16[8,256,256]{1,2,0:T(8,128)(2,1)} %get-tuple-element.587) | copy-start | bytes 3145732
  588.6 12.4 %copy-start.23 = (f32[8,256,64]{1,2,0:T(8,128)S(1)}, f32[8,256,64]{1,2,0:T(8,128)}, u32[]{:S(2)}) copy-start(f32[8,256,64]{1,2,0:T(8,128)} %fusion.166) | copy-start | bytes 1572868
  588.6 12.4 %copy-start.26 = (bf16[256,512]{0,1:T(8,128)(2,1)S(1)}, bf16[256,512]{0,1:T(8,128)(2,1)}, u32[]{:S(2)}) copy-start(bf16[256,512]{0,1:T(8,128)(2,1)} %copy.163) | copy-start | bytes 786436
  672.8 142.6 %copy-start.3 = (f32[4,128,128]{2,1,0:T(8,128)S(1)}, f32[4,128,128]{2,1,0:T(8,128)}, u32[]{:S(2)}) copy-start(f32[4,128,128]{2,1,0:T(8,128)} %custom-call.6) | copy-start | bytes 786436
  721.1 16.8 %copy-start.6 = (f32[8,256,64]{1,2,0:T(8,128)S(1)}, f32[8,256,64]{1,2,0:T(8,128)}, u32[]{:S(2)}) copy-start(f32[8,256,64]{1,2,0:T(8,128)} %get-tuple-element.901) | copy-start | bytes 1572868 | tf_op jit(solution)/shard_map/while
  790.2 16.8 %copy-start.6 = (f32[8,256,64]{1,2,0:T(8,128)S(1)}, f32[8,256,64]{1,2,0:T(8,128)}, u32[]{:S(2)}) copy-start(f32[8,256,64]{1,2,0:T(8,128)} %get-tuple-element.901) | copy-start | bytes 1572868 | tf_op jit(solution)/shard_map/while
  814.2 23.5 %copy-start.22 = (f32[4,4,64,128]{3,2,0,1:T(8,128)S(1)}, f32[4,4,64,128]{3,2,0,1:T(8,128)}, u32[]{:S(2)}) copy-start(f32[4,4,64,128]{3,2,0,1:T(8,128)} %custom-call.7) | copy-start | bytes 1572868
  837.7 24.5 %copy-start.35 = (f32[128]{0:T(128)S(1)}, f32[128]{0:T(128)}, u32[]{:S(2)}) copy-start(f32[128]{0:T(128)} %param.41) | copy-start | bytes 1540
  864.8 156.1 %copy-start.1 = (bf16[2048,8]{0,1:T(8,128)(2,1)S(1)}, bf16[2048,8]{0,1:T(8,128)(2,1)}, u32[]{:S(2)}) copy-start(bf16[2048,8]{0,1:T(8,128)(2,1)} %param.35) | copy-start | bytes 98308
  (14 other events, 32.4 us)
Sparse Core Ops, SparseCore 0:
  10.1 63.1 all-gather.20
  76.0 59.1 all-gather.22
  138.0 61.3 all-gather.14
  202.0 65.1 all-gather.16
  269.8 58.7 all-gather.12
  331.3 59.1 all-gather.24
  393.3 87.2 all-gather.28
  483.3 89.2 all-gather.30
  575.3 145.4 all-gather.26
  723.4 69.9 all-gather.18
  868.3 152.5 reduce-scatter.1
where the time goes:
time: 1040 us; the launch traced here: 1030 us
  waiting for transfers between devices  476 us (46%)
  other arithmetic  272 us (26%)
  matrix products  137 us (13%)
  local copies, waits for them, and re-layouts  87.9 us (8%)
  starting transfers between devices  35.9 us (3%)
  between operations  14.8 us (1%)
    reduce_scatter x1, waiting for transfers between devices, local(): lax.psum_scatter((result + jnp.einsum('hrd,hdn->rn', delta_mixed, delta_w...  153 us
    another operation x12, other arithmetic  91.4 us
    another operation x1, other arithmetic, delta_parts(): jax.scipy.linalg.solve_triangular(jnp.eye(width, dtype=jnp.float32) + str...  79.4 us
    ppermute x8, waiting for transfers between devices, from_behind(): return lax.ppermute(value, axis, pairs)  71.7 us
    all_gather x1, waiting for transfers between devices, local(): lax.all_gather(w_value_delta, 'sp', axis=0, tiled=True)  58.7 us
    all_gather x1, waiting for transfers between devices, local(): lax.all_gather(w_query_delta, 'sp', axis=0, tiled=True)  58.7 us
    all_gather x1, waiting for transfers between devices, local(): lax.all_gather(w_query_attn, 'sp', axis=0, tiled=True)  54.9 us
    all_gather x1, waiting for transfers between devices, local(): lax.all_gather(w_key_delta, 'sp', axis=0, tiled=True)  54.2 us
  transfers between devices with their start and end apart: 19, of which 9 were waited for; matrix products, arithmetic and copies ran while one was open for 47% of the time, Pallas kernels for 0%

commit v1 on v0

v1 whole, which is shorter than its diff:
```python
import functools

import jax
import jax.numpy as jnp
from jax import lax
from jax.experimental import pallas as pl
from jax.experimental.pallas import tpu as pltpu
from jax.sharding import PartitionSpec as P

SB_DIM = 64
GDN_DIM = 128

VMEM = pltpu.VMEM
SMEM = pltpu.SMEM


def layer_normed(tok_rows, ln_gain):
    values = tok_rows.astype(jnp.float32)
    center = jnp.mean(values, axis=-1, keepdims=True)
    spread = jnp.mean(jnp.square(values - center), axis=-1, keepdims=True)
    return ((values - center) * lax.rsqrt(spread + 1e-05) * ln_gain).astype(jnp.bfloat16)


def unit_rows(values):
    return values * lax.rsqrt(jnp.sum(jnp.square(values), axis=-1, keepdims=True) + 1e-06)


def split2(a):
    high = a.astype(jnp.bfloat16)
    return high, (a - high.astype(jnp.float32)).astype(jnp.bfloat16)


def dot_f32(a, b, dims):
    return lax.dot_general(a, b, (dims, ((), ())), preferred_element_type=jnp.float32)


NN = ((1,), (0,))
NT = ((1,), (1,))
TN = ((0,), (0,))


def dot3(a, b, dims=NN):
    ah, al = split2(a)
    bh, bl = split2(b)
    return dot_f32(ah, bh, dims) + (dot_f32(ah, bl, dims) + dot_f32(al, bh, dims))


def stick_kernel(rows, part, off_ref, bias_ref, gain_ref, got_ref, out_ref):
    index = pl.program_id(0)
    queries = got_ref[index, rows : rows + part, :]
    bias = bias_ref[0]
    later = lax.broadcasted_iota(jnp.int32, (rows, rows), 0) > lax.broadcasted_iota(
        jnp.int32, (rows, rows), 1
    )
    later = jnp.where(later, 1.0, 0.0).astype(jnp.bfloat16)

    def turn(block, carry, visible=None):
        acc, kept = carry
        both = got_ref[block, 0:rows, :]
        z = dot_f32(queries, both, NT) * SB_DIM ** (-0.5) + bias
        tail = jnp.log(1.0 + jnp.exp(-jnp.abs(z)))
        lost = -(jnp.maximum(z, 0.0) + tail)
        if visible is not None:
            lost = jnp.where(visible, lost, 0.0)
        high, low = split2(lost)
        between = dot_f32(high, later, NN) + dot_f32(low, later, NN)
        weight = jnp.exp((jnp.minimum(z, 0.0) - tail) + between + kept)
        if visible is not None:
            weight = jnp.where(visible, weight, 0.0)
        acc = acc + dot_f32(weight.astype(jnp.bfloat16), both, NN)
        return acc, kept + (between[:, 0:1] + lost[:, 0:1])

    seen = lax.broadcasted_iota(jnp.int32, (part, rows), 1) < lax.broadcasted_iota(
        jnp.int32, (part, rows), 0
    ) + off_ref[0]
    carry = (jnp.zeros((part, 2 * SB_DIM), jnp.float32), jnp.zeros((part, 1), jnp.float32))
    carry = turn(index, carry, seen)
    odd = lax.rem(index, 2)
    carry = lax.fori_loop(0, odd, lambda step, c: turn(index - 1, c), carry)

    def pair(step, c):
        last = index - odd - 1 - 2 * step
        return turn(last - 1, turn(last, c))

    acc, _ = lax.fori_loop(0, lax.div(index, 2), pair, carry)
    lane = lax.broadcasted_iota(jnp.int32, acc.shape, 1)
    square = jnp.sum(jnp.where(lane >= SB_DIM, acc * acc, 0.0), axis=-1, keepdims=True)
    out = acc * lax.rsqrt(square * (1.0 / SB_DIM) + 1e-06) * gain_ref[...]
    out_ref[0] = out.astype(jnp.bfloat16)


def delta_kernel(q_ref, k_ref, v_ref, col_ref, row_ref, from_ref, own_ref, map_ref):
    rows, width = q_ref.shape
    silu = lambda ref: jax.nn.silu(ref[...].astype(jnp.float32))
    query = unit_rows(silu(q_ref)) * width ** (-0.5)
    key = unit_rows(silu(k_ref))
    value = silu(v_ref)
    beta = col_ref[0, :, 0:1]
    g_col = col_ref[0, :, 1:2]
    g_row = row_ref[0]
    ii = lax.broadcasted_iota(jnp.int32, (rows, rows), 0)
    jj = lax.broadcasted_iota(jnp.int32, (rows, rows), 1)
    lower = ii >= jj
    sum_col = jnp.sum(jnp.where(lower, g_row, 0.0), axis=1, keepdims=True)
    sum_row = jnp.sum(jnp.where(ii <= jj, g_col, 0.0), axis=0, keepdims=True)
    end = sum_col[rows - 1 : rows, :]
    decay_mask = jnp.where(lower, jnp.exp(jnp.where(lower, sum_col - sum_row, 0.0)), 0.0)
    key_beta = key * beta
    strict = jnp.where(ii > jj, dot3(key_beta, key, NT) * decay_mask, 0.0)
    inverse = jnp.where(
        ii == jj, 1.0, jnp.where((ii >> 1) == (jj >> 1), -strict, 0.0)
    )
    level = 1
    while (1 << level) < rows:
        joined = (ii >> (level + 1)) == (jj >> (level + 1))
        apart = (ii >> level) != (jj >> level)
        corner = jnp.where(joined & apart, strict, 0.0)
        inverse = inverse - dot3(dot3(inverse, corner), inverse)
        level += 1
    grown = jnp.exp(sum_col)
    solved = dot3(inverse, jnp.concatenate([key_beta * grown, value * beta], axis=1))
    query_key = dot3(query, key, NT) * decay_mask
    mixed = dot3(query_key, solved)
    from_ref[...] = query * grown - mixed[:, :width]
    own_ref[...] = mixed[:, width:]
    map_ref[0] = dot3(key * jnp.exp(end - sum_col), solved, TN).astype(jnp.bfloat16)


def state_kernel(heads, pos_ref, decay_ref, gain_ref, maps_ref, from_ref, own_ref, out_ref):
    width = gain_ref.shape[1]

    def turn(block, states):
        new = []
        for head, state in enumerate(states):
            high, low = split2(state)
            both = maps_ref[block, head]
            taken = both[:, :width]
            moved = dot_f32(taken, high, NN) + dot_f32(taken, low, NN)
            new.append(
                state * decay_ref[block, head] - moved + both[:, width:].astype(jnp.float32)
            )
        return tuple(new)

    zero = jnp.zeros((width, width), jnp.float32)
    states = lax.fori_loop(0, pos_ref[0], turn, (zero,) * heads)
    for head, state in enumerate(states):
        cols = slice(head * width, (head + 1) * width)
        raw = dot3(from_ref[:, cols], state) + own_ref[:, cols]
        scale = lax.rsqrt(jnp.mean(raw * raw, axis=-1, keepdims=True) + 1e-06)
        out_ref[:, cols] = (raw * scale * gain_ref[...]).astype(jnp.bfloat16)


def local(
    tokens,
    ln_gain,
    w_query_attn,
    w_key_attn,
    w_value_attn,
    w_query_delta,
    w_key_delta,
    w_value_delta,
    w_beta,
    w_decay,
    attn_bias,
    decay_log,
    beta_bias,
    log_decay_extra,
    attn_gain,
    delta_gain,
    w_out_attn,
    w_out_delta,
):
    rows = tokens.shape[0]
    sp_size = lax.axis_size("sp")
    tp_pos = lax.axis_index("tp")
    sp_pos = lax.axis_index("sp")
    heads = w_query_attn.shape[1] // SB_DIM
    delta_heads = w_query_delta.shape[1] // GDN_DIM
    group = sp_size // heads
    part = rows // group
    depth = w_query_attn.shape[0]

    w_delta = jnp.concatenate([w_query_delta, w_key_delta, w_value_delta], axis=1)
    w_pairs = jnp.concatenate(
        [w_key_attn.reshape(depth, heads, SB_DIM), w_value_attn.reshape(depth, heads, SB_DIM)],
        axis=2,
    ).reshape(depth, 2 * heads * SB_DIM)
    w_attn = jnp.concatenate([w_pairs, w_query_attn], axis=1)
    w_delta = lax.all_gather(w_delta, "sp", axis=0, tiled=True)
    w_attn = lax.all_gather(w_attn, "sp", axis=0, tiled=True)

    normed = layer_normed(tokens, ln_gain)
    project = lambda w: jnp.dot(normed, w, preferred_element_type=jnp.float32).astype(jnp.bfloat16)

    first = tp_pos * delta_heads
    mine = lambda a, axis: lax.dynamic_slice_in_dim(a, first, delta_heads, axis)
    gates = project(jnp.concatenate([mine(w_beta, 1), mine(w_decay, 1)], axis=1))
    gates = gates.astype(jnp.float32)
    beta = jax.nn.sigmoid(gates[:, :delta_heads] + mine(beta_bias, 0))
    rates = jnp.exp(mine(decay_log, 0))
    decay = -rates * jax.nn.softplus(gates[:, delta_heads:]) + log_decay_extra
    block_decay = lax.all_gather(jnp.exp(jnp.sum(decay, axis=0)), "sp", axis=0)
    cols = jnp.transpose(jnp.stack([beta, decay], axis=2), (1, 0, 2))
    g_rows = jnp.transpose(decay)[:, None, :]

    delta_all = project(w_delta)
    head_cols = lambda base: pl.BlockSpec((rows, GDN_DIM), lambda h: (0, base + h))
    wide = delta_heads * GDN_DIM
    from_state, own, maps = pl.pallas_call(
        delta_kernel,
        grid=(delta_heads,),
        in_specs=[
            head_cols(0),
            head_cols(delta_heads),
            head_cols(2 * delta_heads),
            pl.BlockSpec((1, rows, 2), lambda h: (h, 0, 0)),
            pl.BlockSpec((1, 1, rows), lambda h: (h, 0, 0)),
        ],
        out_specs=[
            head_cols(0),
            head_cols(0),
            pl.BlockSpec((1, GDN_DIM, 2 * GDN_DIM), lambda h: (h, 0, 0)),
        ],
        out_shape=[
            jax.ShapeDtypeStruct((rows, wide), jnp.float32),
            jax.ShapeDtypeStruct((rows, wide), jnp.float32),
            jax.ShapeDtypeStruct((delta_heads, GDN_DIM, 2 * GDN_DIM), jnp.bfloat16),
        ],
        cost_estimate=pl.CostEstimate(
            flops=delta_heads * 120 * rows**3, bytes_accessed=4 * rows * wide, transcendentals=0
        ),
        name="delta_blocks",
    )(delta_all, delta_all, delta_all, cols, g_rows)
    maps = lax.all_gather(maps, "sp", axis=0)

    attn_all = project(w_attn)
    pair_wide = 2 * heads * SB_DIM
    pairs = jnp.transpose(attn_all[:, :pair_wide].reshape(rows, heads, 2 * SB_DIM), (1, 0, 2))
    queries = attn_all[:, pair_wide:].reshape(group, part, heads, SB_DIM)
    queries = jnp.transpose(queries, (2, 0, 1, 3))
    queries = jnp.pad(queries, ((0, 0), (0, 0), (0, 0), (0, SB_DIM)))
    pairs = jnp.broadcast_to(pairs[:, None], (heads, group, rows, 2 * SB_DIM))
    sent = jnp.concatenate([pairs, queries], axis=2).reshape(sp_size, rows + part, 2 * SB_DIM)
    got = lax.all_to_all(sent, "sp", 0, 0, tiled=True)
    bias = lax.dynamic_slice_in_dim(attn_bias, tp_pos * heads + sp_pos // group, 1, 0)
    offset = (lax.rem(sp_pos, group) * part).astype(jnp.int32)[None]
    gain = jnp.concatenate([jnp.zeros_like(attn_gain), attn_gain])[None]
    mixed = pl.pallas_call(
        functools.partial(stick_kernel, rows, part),
        grid=(sp_size,),
        in_specs=[
            pl.BlockSpec(memory_space=SMEM),
            pl.BlockSpec(memory_space=SMEM),
            pl.BlockSpec(memory_space=VMEM),
            pl.BlockSpec(memory_space=VMEM),
        ],
        out_specs=pl.BlockSpec((1, part, 2 * SB_DIM), lambda i: (i, 0, 0)),
        out_shape=jax.ShapeDtypeStruct((sp_size, part, 2 * SB_DIM), jnp.bfloat16),
        cost_estimate=pl.CostEstimate(
            flops=sp_size * sp_size * rows * part * 20000,
            bytes_accessed=sp_size * rows * 512,
            transcendentals=0,
        ),
        name="stick_attention",
    )(offset, bias, gain, got)
    back = lax.all_to_all(mixed[:, :, SB_DIM:], "sp", 0, 0, tiled=True)
    back = back.reshape(heads, group, part, SB_DIM)
    attn_cols = jnp.transpose(back, (1, 2, 0, 3)).reshape(rows, heads * SB_DIM)

    delta_cols = pl.pallas_call(
        functools.partial(state_kernel, delta_heads),
        in_specs=[pl.BlockSpec(memory_space=SMEM)] * 2 + [pl.BlockSpec(memory_space=VMEM)] * 4,
        out_specs=pl.BlockSpec(memory_space=VMEM),
        out_shape=jax.ShapeDtypeStruct((rows, wide), jnp.bfloat16),
        cost_estimate=pl.CostEstimate(
            flops=sp_size * wide * GDN_DIM * 10000, bytes_accessed=8 * rows * wide, transcendentals=0
        ),
        name="delta_state",
    )(sp_pos.astype(jnp.int32)[None], block_decay, delta_gain[None], maps, from_state, own)

    w_out = lax.all_gather(
        jnp.concatenate([w_out_attn, w_out_delta], axis=0), "sp", axis=1, tiled=True
    )
    joined = jnp.concatenate([attn_cols, delta_cols], axis=1)
    result = jnp.dot(joined, w_out, preferred_element_type=jnp.float32).astype(jnp.bfloat16)
    return lax.psum_scatter(result, "tp", scatter_dimension=0, tiled=True)


def solution(mesh):
    in_specs = (
        P("sp", None),
        P(),
        P("sp", "tp"),
        P("sp", "tp"),
        P("sp", "tp"),
        P("sp", "tp"),
        P("sp", "tp"),
        P("sp", "tp"),
        P(),
        P(),
        P(),
        P(),
        P(),
        P("sp", "tp"),
        P(),
        P(),
        P("tp", "sp"),
        P("tp", "sp"),
    )
    out_specs = P(("sp", "tp"), None)
    return jax.shard_map(local, mesh=mesh, in_specs=in_specs, out_specs=out_specs, check_vma=False)
```

time: 1040 us -> 433 us (0.42); the launches traced: 1030 us -> 433 us
  other arithmetic: 272 us -> 6.22 us
  waiting for transfers between devices: 476 us -> 236 us
  matrix products: 137 us -> 15.2 us
  Pallas kernels: 0 us -> 91 us
  local copies, waits for them, and re-layouts: 87.9 us -> 12.2 us
  blocking collectives: 0 us -> 43.5 us
  starting transfers between devices: 35.9 us -> 15 us
    another operation x20 -> x0, other arithmetic: 190 us -> none
    reduce_scatter x1, waiting for transfers between devices: 153 us -> 6.82 us  [local(): return lax.psum_scatter(result, 'tp', scatter_dimension=0, tiled=True)]
    dot_general x71 -> x4, matrix products: 136 us -> 15.2 us  [the longest x3 10.7 us: local(): jnp.dot(normed, w, preferred_element_type=jnp.float32).astype(jnp.bfloat16)]
    pallas_call x0 -> x3, Pallas kernels: none -> 91 us  [the longest x1 66.2 us: local(): pl.pallas_call(functools.partial(stick_kernel, rows, part), grid=(sp_size...]
    ppermute x8 -> x0, waiting for transfers between devices: 71.7 us -> none  [from_behind(): return lax.ppermute(value, axis, pairs)]
    all_gather x10 -> x4, waiting for transfers between devices: 246 us -> 184 us  [the longest x1 90 us: local(): w_delta = lax.all_gather(w_delta, 'sp', axis=0, tiled=True)]
    another operation x20 -> x0, local copies, waits for them, and re-layouts: 46.6 us -> none  [the longest x7 30.6 us: stick_block(): lax.cumsum(lost, axis=2, reverse=True) - lost + log_kept[:, :, None]]
    all_to_all x0 -> x2, waiting for transfers between devices: none -> 44.6 us  [the longest x1 44.6 us: local(): got = lax.all_to_all(sent, 'sp', 0, 0, tiled=True)]
  transfers between devices with their start and end apart: 19 -> 7, of which waited for: 9 -> 5; matrix products, arithmetic and copies ran while one was open for 47% -> 6% of each run, Pallas kernels for 0% -> 21%
where the time goes in v1:
time: 433 us
  waiting for transfers between devices  236 us (55%)
  Pallas kernels  91 us (21%)
  blocking collectives  43.5 us (10%)
  matrix products  15.2 us (4%)
  starting transfers between devices  15 us (3%)
  between operations  14.1 us (3%)
  local copies, waits for them, and re-layouts  12.2 us (3%)
  other arithmetic  6.22 us (1%)
    all_gather x1, waiting for transfers between devices, local(): w_delta = lax.all_gather(w_delta, 'sp', axis=0, tiled=True)  90 us
    all_gather x1, waiting for transfers between devices, local(): w_attn = lax.all_gather(w_attn, 'sp', axis=0, tiled=True)  89.6 us
    pallas_call x1, Pallas kernels, local(): pl.pallas_call(functools.partial(stick_kernel, rows, part), grid=(sp_size...  66.2 us
    all_to_all x1, waiting for transfers between devices, local(): got = lax.all_to_all(sent, 'sp', 0, 0, tiled=True)  44.6 us
    unnamed x1, blocking collectives  43.5 us
    pallas_call x1, Pallas kernels, local(): pl.pallas_call(delta_kernel, grid=(delta_heads,), in_specs=[head_cols(0),...  21.2 us
    all_to_all x1, starting transfers between devices, local(): back = lax.all_to_all(mixed[:, :, SB_DIM:], 'sp', 0, 0, tiled=True)  10.9 us
    dot_general x3, matrix products, local(): jnp.dot(normed, w, preferred_element_type=jnp.float32).astype(jnp.bfloat16)  10.7 us
  transfers between devices with their start and end apart: 7, of which 5 were waited for; matrix products, arithmetic and copies ran while one was open for 6% of the time, Pallas kernels for 21%

profile of v1, /device:TPU:0, one launch (start us, length us, event | category | flops | bytes accessed | tf_op | source)
XLA Modules:
  0.0 432.9 jit_solution(15838121024890376722)
XLA Ops:
  6.5 1.9 pad_maximum_fusion.1
  8.5 0.0 all-gather.7.cloned.1.call-start
  8.5 1.0 copy.32
  9.6 1.0 copy.33
  10.6 1.0 copy.34
  11.7 0.8 pad_maximum_fusion
  12.5 0.0 all-gather.13.cloned.1.call-start
  12.6 0.1 dynamic_slice.19
  12.6 0.1 exponential_negate_fusion
  12.7 0.2 convert_reduce_fusion
  13.0 0.4 fusion.3
  13.5 0.5 fusion.7
  14.0 0.7 fusion.26
  14.6 1.0 copy.40.col_ref
  15.7 0.6 broadcast_in_dim.32.row_ref
  16.3 90.0 %all-gather.9.cloned.1.call-done = bf16[2048,1536]{1,0:T(8,128)(2,1)} async-done(((bf16[128,1536]{1,0:T(8,128)(2,1)}), bf16[2048,1536]{1,0:T(8,128)(2,1)}) %all-gather.9.cloned.1.call-update) | async-done | bytes 6291472 | tf_op jit(solution)/shard_map/all_gather | solution.py:189
  106.3 5.6 %convolution_convert_fusion.1.q_ref.k_ref.v_ref = bf16[256,1536]{1,0:T(8,128)(2,1)} fusion(bf16[2048,1536]{1,0:T(8,128)(2,1)} %all-gather.9.cloned.1.call-done, bf16[256,2048]{1,0:T(8,128)(2,1)S(1)} %copy-done, f32[2048]{0:T(1024)S(1)} %copy-done.8, f32[256]{0:T(256)S(1)} %add_rsqrt_fusion, f32[256]{0:T(256)S(1)} %broadcast_multiply_fusion), kind=kOutput, calls=%fused_computation.5 | convolution fusion | flops 1613627392 | bytes 8136704 | tf_op jit(solution)/shard_map/dot_general | solution.py:193
  111.8 21.2 %delta_blocks.1 = (f32[256,512]{1,0:T(8,128)}, f32[256,512]{1,0:T(8,128)}, bf16[4,128,256]{2,1,0:T(8,128)(2,1)}) custom-call(bf16[256,1536]{1,0:T(8,128)(2,1)} %convolution_convert_fusion.1.q_ref.k_ref.v_ref, bf16[256,1536]{1,0:T(8,128)(2,1)} %convolution_convert_fusion.1.q_ref.k_ref.v_ref, bf16[256,1536]{1,0:T(8,128)(2,1)} %convolution_convert_fusion.1.q_ref.k_ref.v_ref, ...), custom_call_target="tpu_custom_call" | custom-call | flops 8053063680 | bytes 524288 | tf_op jit(solution)/shard_map/delta_blocks/pallas_call | solution.py:209
  133.0 89.6 %all-gather.7.cloned.1.call-done = bf16[2048,1536]{0,1:T(8,128)(2,1)} async-done(((bf16[128,1536]{0,1:T(8,128)(2,1)}), bf16[2048,1536]{0,1:T(8,128)(2,1)}) %all-gather.7.cloned.1.call-update) | async-done | bytes 6291472 | tf_op jit(solution)/shard_map/all_gather | solution.py:190
  222.7 4.6 %convolution_convert_fusion.2 = bf16[256,1536]{1,0:T(8,128)(2,1)S(1)} fusion(bf16[2048,1536]{0,1:T(8,128)(2,1)} %all-gather.7.cloned.1.call-done, bf16[256,2048]{1,0:T(8,128)(2,1)S(1)} %copy-done, f32[2048]{0:T(1024)S(1)} %copy-done.8, f32[256]{0:T(256)S(1)} %add_rsqrt_fusion, f32[256]{0:T(256)S(1)} %broadcast_multiply_fusion), kind=kOutput, calls=%fused_computation.6 | convolution fusion | flops 1613627392 | bytes 8136704 | tf_op jit(solution)/shard_map/dot_general | solution.py:193
  227.3 0.1 slice_bitcast_fusion
  227.4 0.1 copy.43
  227.5 0.1 copy.35
  227.6 0.1 copy.36
  227.7 0.1 reshape.52
  227.8 0.3 copy.42
  228.1 0.2 broadcast_in_dim.14
  228.3 1.4 fusion.6
  229.7 3.9 all-to-all-start
  233.7 0.7 pad_maximum_fusion.3
  234.5 0.6 dynamic_slice.15.bias_ref
  235.0 0.6 pad_bitcast_fusion.gain_ref
  235.6 44.6 %all-to-all-done.got_ref = bf16[16,384,128]{2,1,0:T(8,128)(2,1)S(1)} async-done(((bf16[16,384,128]{2,1,0:T(8,128)(2,1)}), bf16[16,384,128]{2,1,0:T(8,128)(2,1)S(1)}, u32[]{:S(2)}, u32[]{:S(2)}) %all-to-all-start) | async-done | bytes 1572896 | tf_op jit(solution)/shard_map/all_to_all | solution.py:244
  280.2 1.2 copy-done.1
  281.4 66.2 %stick_attention.1 = bf16[16,128,128]{2,1,0:T(8,128)(2,1)} custom-call(s32[1]{0:T(128)} %bitcast.off_ref, f32[1]{0:T(128)} %dynamic_slice.15.bias_ref, f32[1,128]{1,0:T(1,128)} %pad_bitcast_fusion.gain_ref, bf16[16,384,128]{2,1,0:T(8,128)(2,1)} %copy-done.1), custom_call_target="tpu_custom_call" | custom-call | flops 167772160000 | bytes 2097152 | tf_op jit(solution)/shard_map/stick_attention/pallas_call | solution.py:248
  347.5 1.3 slice.22
  348.8 0.9 copy.38
  349.7 10.9 %all-to-all-start.1 = ((bf16[16,128,64]{1,2,0:T(8,128)(2,1)}), bf16[16,128,64]{1,2,0:T(8,128)(2,1)S(1)}, u32[]{:S(2)}, u32[]{:S(2)}) async-start(bf16[16,128,64]{1,2,0:T(8,128)(2,1)} %copy.38), calls=%async_computation.1 | async-start | bytes 524288 | tf_op jit(solution)/shard_map/all_to_all | solution.py:266
  360.7 0.6 dynamic-slice
  362.0 0.1 exponential_dynamic-update-slice_fusion
  362.1 43.5 %all-reduce.2 = f32[64]{0:T(128)S(1)} all-reduce(f32[64]{0:T(128)S(1)} %exponential_dynamic-update-slice_fusion), channel_id=2, replica_groups=mesh['sp'=16,'tp'=2] {'sp'}, use_global_device_ids=true, to_apply=%add.2 | all-reduce | flops 64 | bytes 512
  405.6 0.7 reshape.56.decay_ref
  406.3 0.3 copy.39
  406.6 0.1 copy.41
  406.8 3.7 delta_state.1
  410.5 4.6 %all-gather.11.cloned.1.call-done = bf16[1024,2048]{1,0:T(8,128)(2,1)} async-done(((bf16[1024,128]{1,0:T(8,128)(2,1)}), bf16[1024,2048]{1,0:T(8,128)(2,1)}) %all-gather.11.cloned.1.call-update) | async-done | bytes 4194320 | tf_op jit(solution)/shard_map/all_gather | solution.py:281
  415.0 4.5 %convolution_convert_fusion = bf16[256,2048]{1,0:T(8,128)(2,1)} fusion(bf16[1024,2048]{1,0:T(8,128)(2,1)} %all-gather.11.cloned.1.call-done, bf16[256,512]{1,0:T(8,128)(2,1)} %delta_state.1, bf16[256,512]{1,0:T(8,128)(2,1)S(1)} %copy.41), kind=kOutput, calls=%fused_computation.4 | convolution fusion | flops 1075314688 | bytes 5767168 | tf_op jit(solution)/shard_map/dot_general | solution.py:285
  419.6 6.8 %reduce-scatter.2.cloned.1.call-done = bf16[128,2048]{1,0:T(8,128)(2,1)} async-done(((bf16[256,2048]{1,0:T(8,128)(2,1)}), bf16[128,2048]{1,0:T(8,128)(2,1)}) %reduce-scatter.2.cloned.1.call-update) | async-done | bytes 524304 | tf_op jit(solution)/shard_map/reduce_scatter | solution.py:286
  (45 shorter events, 0.4 us)
Async XLA Ops:
  6.5 6.0 %copy-start.9 = (f32[8]{0:T(128)S(1)}, f32[8]{0:T(128)}, u32[]{:S(2)}) copy-start(f32[8]{0:T(128)} %param.30) | copy-start | bytes 100
  6.5 6.1 %copy-start.10 = (f32[8]{0:T(128)S(1)}, f32[8]{0:T(128)}, u32[]{:S(2)}) copy-start(f32[8]{0:T(128)} %param.29) | copy-start | bytes 100
  6.5 6.2 %copy-start = (bf16[256,2048]{1,0:T(8,128)(2,1)S(1)}, bf16[256,2048]{1,0:T(8,128)(2,1)}, u32[]{:S(2)}) copy-start(bf16[256,2048]{1,0:T(8,128)(2,1)} %param.18) | copy-start | bytes 3145732
  6.5 99.7 %all-gather.9.cloned.1.call-start = ((), (), s32[]{:S(2)}) async-start(), calls=%async_computation.4 | async-start | bytes 6684672 | tf_op jit(solution)/shard_map/all_gather | solution.py:189
  8.5 214.2 %all-gather.7.cloned.1.call-start = ((), (), s32[]{:S(2)}) async-start(), calls=%async_computation.3 | async-start | bytes 6684672 | tf_op jit(solution)/shard_map/all_gather | solution.py:190
  10.6 2.8 copy-start.4
  10.6 2.8 copy-start.5
  10.6 2.8 copy-start.8
  12.5 394.3 %all-gather.13.cloned.1.call-start = ((), (), s32[]{:S(2)}) async-start(), calls=%async_computation.7 | async-start | bytes 4456448 | tf_op jit(solution)/shard_map/all_gather | solution.py:234
  12.7 1.2 copy-start.6
  229.7 4.0 copy-start.2
  229.7 4.0 copy-start.3
  229.7 4.8 %copy-start.11 = (f32[16]{0:T(128)S(1)}, f32[16]{0:T(128)}, u32[]{:S(2)}) copy-start(f32[16]{0:T(128)} %param.28) | copy-start | bytes 196
  229.7 5.3 %copy-start.12 = (f32[64]{0:T(128)S(1)}, f32[64]{0:T(128)}, u32[]{:S(2)}) copy-start(f32[64]{0:T(128)} %param.32) | copy-start | bytes 772
  229.7 50.5 %all-to-all-start = ((bf16[16,384,128]{2,1,0:T(8,128)(2,1)}), bf16[16,384,128]{2,1,0:T(8,128)(2,1)S(1)}, u32[]{:S(2)}, u32[]{:S(2)}) async-start(bf16[16,384,128]{2,1,0:T(8,128)(2,1)} %bitcast.7), calls=%async_computation | async-start | bytes 3145728 | tf_op jit(solution)/shard_map/all_to_all | solution.py:244
  233.6 181.4 %all-gather.11.cloned.1.call-start = ((), (), s32[]{:S(2)}) async-start(), calls=%async_computation.5 | async-start | bytes 4456448 | tf_op jit(solution)/shard_map/all_gather | solution.py:281
  280.2 1.2 copy-start.1
  347.5 13.2 %copy-start.13 = (u32[32]{0:T(128)S(1)}, u32[32]{0:T(128)}, u32[]{:S(2)}) copy-start(u32[32]{0:T(128)} %constant.52) | copy-start | bytes 388
  347.5 14.4 %copy-start.7 = (f32[4]{0:T(128)S(1)}, f32[4]{0:T(128)}, u32[]{:S(2)}) copy-start(f32[4]{0:T(128)} %get-tuple-element.11) | copy-start | bytes 52
  349.7 56.6 %all-to-all-start.1 = ((bf16[16,128,64]{1,2,0:T(8,128)(2,1)}), bf16[16,128,64]{1,2,0:T(8,128)(2,1)S(1)}, u32[]{:S(2)}, u32[]{:S(2)}) async-start(bf16[16,128,64]{1,2,0:T(8,128)(2,1)} %copy.38), calls=%async_computation.1 | async-start | bytes 524288 | tf_op jit(solution)/shard_map/all_to_all | solution.py:266
  360.6 65.8 %reduce-scatter.2.cloned.1.call-start = ((), (), s32[]{:S(2)}) async-start(), calls=%async_computation.6 | async-start | bytes 1572864 | tf_op jit(solution)/shard_map/reduce_scatter | solution.py:286
Sparse Core Ops, SparseCore 0:
  10.1 96.1 all-gather.8
  109.0 113.6 all-gather.6
  225.4 93.7 all-gather.12
  321.8 93.2 all-gather.10
  419.7 6.6 reduce-scatter.1
